TPU v7x, 32 devices: a whole 2x2x4 slice. The times are simulated.
32 devices in a mesh: ra: 4 (over y, x), cb: 8 (over z, core).
Axes of the slice: x: 2, y: 2, z: 4, core: 2. Of those that a mesh axis runs over, the one named last changes fastest.
Arguments:
- tokens: bfloat16 [256, 4096], P(None, 'ra'), may hold values from -20 to 20, as said below
- norm_gain: float32 [2, 4096], P(None, 'ra'), may hold values from 0.1 to 1.9
- gate_weight: bfloat16 [2, 4096, 11008], P(None, 'ra', 'cb'), may hold values from -0.09375 to 0.09375
- value_weight: bfloat16 [2, 4096, 11008], P(None, 'ra', 'cb'), may hold values from -0.09375 to 0.09375
- gate_taps: float32 [2, 3, 11008], P(None, None, 'cb'), may hold values from -3.5 to 3.5
- value_taps: float32 [2, 3, 11008], P(None, None, 'cb'), may hold values from -3.5 to 3.5
- down_weight: bfloat16 [2, 11008, 4096], P(None, 'cb', 'ra'), may hold values from -0.0546875 to 0.0546875
Outputs:
- mixed: bfloat16 [256, 4096], P(None, 'ra')
Inputs may be any that keep to these rules, and one draw needn't show every extreme that they name: tokens have features drawn around zero with a scale that varies by blocks of features between about 0.3 and 3.3.
All inputs are finite; a program needn't handle non-finite values.
Results may differ from a plain program's by a relative error of at most 0.0075.
Values may be sent and summed in bfloat16 or wider, within the bound.
A program may use at most 128 MiB of HBM per device.

v0:
```python
import jax
import jax.numpy as jnp
from jax import lax
from jax.sharding import PartitionSpec as P

D = 4096


epsilon = 1e-06


def conv_after(signal, earlier, kernel_taps):
    length = signal.shape[0]
    width = kernel_taps.shape[0]
    padded = jnp.concatenate([earlier, signal], axis=0)
    result = jnp.zeros(signal.shape, jnp.float32)
    for offset in range(width):
        result = result + kernel_taps[offset] * padded[offset : offset + length]
    return result


def causal_conv(signal, kernel_taps):
    width = kernel_taps.shape[0]
    return conv_after(signal, jnp.zeros((width - 1, signal.shape[1]), jnp.float32), kernel_taps)


def body(tokens, norm_gain, gate_weight, value_weight, gate_taps, value_taps, down_weight):
    stream = tokens
    for layer_index in range(gate_weight.shape[0]):
        current = stream.astype(jnp.float32)
        local_squares = jnp.sum(current * current, axis=1, keepdims=True)
        scaled = (current * norm_gain[layer_index]).astype(jnp.bfloat16)
        gate_part = jnp.dot(scaled, gate_weight[layer_index], preferred_element_type=jnp.float32)
        value_part = jnp.dot(scaled, value_weight[layer_index], preferred_element_type=jnp.float32)
        total_squares = lax.psum(local_squares, "ra")
        gate_sum, value_sum = lax.psum((gate_part, value_part), "ra")
        inverse_rms = lax.rsqrt(total_squares / D + epsilon)
        gate_conv = causal_conv(gate_sum * inverse_rms, gate_taps[layer_index])
        value_conv = causal_conv(value_sum * inverse_rms, value_taps[layer_index])
        hidden = (jax.nn.silu(gate_conv) * value_conv).astype(jnp.bfloat16)
        partial_branch = jnp.dot(
            hidden, down_weight[layer_index], preferred_element_type=jnp.float32
        )
        branch = lax.psum(partial_branch, "cb")
        stream = (0.5 * current + branch).astype(jnp.bfloat16)
    return stream


def solution(mesh):
    return jax.shard_map(
        body,
        mesh=mesh,
        in_specs=(
            P(None, "ra"),
            P(None, "ra"),
            P(None, "ra", "cb"),
            P(None, "ra", "cb"),
            P(None, None, "cb"),
            P(None, None, "cb"),
            P(None, "cb", "ra"),
        ),
        out_specs=P(None, "ra"),
        check_vma=False,
    )
```

profile of v0, /device:TPU:0, one launch (start us, length us, event | category | flops | bytes accessed | tf_op | source)
XLA Modules:
  0.0 333.7 jit_solution(11090075387825171046)
XLA Ops:
  6.5 0.0 all-reduce.17.cloned.1.call-start
  6.5 0.8 fusion.57
  7.3 0.0 copy-start
  7.3 4.0 %fusion.8 = f32[256,1376]{0,1:T(8,128)} fusion(bf16[2,1024,1376]{1,2,0:T(8,128)(2,1)} %param.10, bf16[256,1024]{1,0:T(8,128)(2,1)} %param.7, f32[1024]{0:T(1024)S(1)} %bitcast.30), kind=kOutput, calls=%fused_computation.8 | convolution fusion | flops 722206720 | bytes 4755456 | tf_op jit(solution)/shard_map/dot_general | solution.py:34
  11.4 0.0 copy-done
  11.4 3.8 %fusion.10 = f32[256,1376]{0,1:T(8,128)} fusion(bf16[2,1024,1376]{1,2,0:T(8,128)(2,1)} %param.9, bf16[256,1024]{1,0:T(8,128)(2,1)S(1)} %copy-done, f32[1024]{0:T(1024)S(1)} %bitcast.31), kind=kOutput, calls=%fused_computation.10 | convolution fusion | flops 722206720 | bytes 4755456 | tf_op jit(solution)/shard_map/dot_general | solution.py:33
  15.2 0.0 copy-start.1
  15.2 0.0 copy-start.2
  15.2 0.0 all-reduce.17.cloned.1.call-update
  15.2 0.0 all-reduce.11.cloned.1.call-start
  15.3 0.2 fusion.41
  15.5 11.5 %psum.57 = f32[256,1]{0,1:T(1,128)S(1)} all-reduce(f32[256,1]{0,1:T(1,128)S(1)} %bitcast.27), channel_id=1, replica_groups=mesh['ra'=4,'cb'=8] {'ra'}, use_global_device_ids=true, to_apply=%region_2.0 | all-reduce | flops 256 | bytes 2048 | tf_op jit(solution)/shard_map/psum | solution.py:35
  27.0 0.0 copy-done.1
  27.0 0.0 copy-done.2
  27.0 0.2 slice_reduce_fusion.2
  27.1 72.5 %all-reduce.17.cloned.1.call-done = (f32[256,1376]{0,1:T(8,128)}, f32[256,1376]{0,1:T(8,128)}) async-done(((f32[256,1376]{0,1:T(8,128)}, f32[256,1376]{0,1:T(8,128)}), (f32[256,1376]{0,1:T(8,128)}, f32[256,1376]{0,1:T(8,128)})) %all-reduce.17.cloned.1.call-update) | async-done | bytes 2818064 | tf_op jit(solution)/shard_map/psum | solution.py:36
  99.6 2.0 broadcast_multiply_fusion.3
  101.6 6.3 %fusion.6 = f32[256,1024]{1,0:T(8,128)} fusion(bf16[2,1376,1024]{2,1,0:T(8,128)(2,1)} %param.13, f32[256,1376]{0,1:T(8,128)S(1)} %get-tuple-element.28, f32[256,1376]{0,1:T(8,128)S(1)} %get-tuple-element.27, f32[1376]{0:T(1024)S(1)} %get-tuple-element.12, f32[1376]{0:T(1024)S(1)} %get-tuple-element.13, f32[1376]{0:T(1024)S(1)} %get-tuple-element.14, ...), kind=kOutput, calls=%fused_computation.6 | convolution fusion | flops 727056384 | bytes 6717696 | tf_op jit(solution)/shard_map/dot_general | solution.py:41
  107.9 0.0 all-reduce.11.cloned.1.call-update
  107.9 0.0 all-reduce.15.cloned.1.call-start
  107.9 59.4 %all-reduce.11.cloned.1.call-done = f32[256,1024]{1,0:T(8,128)} async-done(((f32[256,1024]{1,0:T(8,128)}), f32[256,1024]{1,0:T(8,128)}) %all-reduce.11.cloned.1.call-update) | async-done | bytes 1048592 | tf_op jit(solution)/shard_map/psum | solution.py:44
  167.3 1.5 fusion.45
  168.8 3.8 %fusion.4 = f32[256,1376]{0,1:T(8,128)} fusion(bf16[2,1024,1376]{1,2,0:T(8,128)(2,1)} %param.9, bf16[256,1024]{1,0:T(8,128)(2,1)S(1)} %get-tuple-element.22, f32[1024]{0:T(1024)S(1)} %bitcast.28), kind=kOutput, calls=%fused_computation.4 | convolution fusion | flops 722206720 | bytes 4755456 | tf_op jit(solution)/shard_map/dot_general | solution.py:33
  172.6 3.8 %fusion.2 = f32[256,1376]{0,1:T(8,128)} fusion(bf16[2,1024,1376]{1,2,0:T(8,128)(2,1)} %param.10, bf16[256,1024]{1,0:T(8,128)(2,1)S(1)} %get-tuple-element.22, f32[1024]{0:T(1024)S(1)} %bitcast.29), kind=kOutput, calls=%fused_computation.2 | convolution fusion | flops 722206720 | bytes 4755456 | tf_op jit(solution)/shard_map/dot_general | solution.py:34
  176.5 0.0 all-reduce.15.cloned.1.call-update
  176.5 0.0 all-reduce.13.cloned.1.call-start
  176.5 10.1 %psum.61 = f32[256,1]{0,1:T(1,128)S(1)} all-reduce(f32[256,1]{0,1:T(1,128)S(1)} %bitcast.24), channel_id=1, replica_groups=mesh['ra'=4,'cb'=8] {'ra'}, use_global_device_ids=true, to_apply=%region_7.8 | all-reduce | flops 256 | bytes 2048 | tf_op jit(solution)/shard_map/psum | solution.py:35
  186.6 70.6 %all-reduce.15.cloned.1.call-done = (f32[256,1376]{0,1:T(8,128)}, f32[256,1376]{0,1:T(8,128)}) async-done(((f32[256,1376]{0,1:T(8,128)}, f32[256,1376]{0,1:T(8,128)}), (f32[256,1376]{0,1:T(8,128)}, f32[256,1376]{0,1:T(8,128)})) %all-reduce.15.cloned.1.call-update) | async-done | bytes 2818064 | tf_op jit(solution)/shard_map/psum | solution.py:36
  257.3 2.0 broadcast_multiply_fusion.1
  259.2 6.3 %fusion = f32[256,1024]{1,0:T(8,128)} fusion(bf16[2,1376,1024]{2,1,0:T(8,128)(2,1)} %param.13, f32[256,1376]{0,1:T(8,128)S(1)} %get-tuple-element.26, f32[256,1376]{0,1:T(8,128)S(1)} %get-tuple-element.25, f32[1376]{0:T(1024)S(1)} %get-tuple-element.15, f32[1376]{0:T(1024)S(1)} %get-tuple-element.16, f32[1376]{0:T(1024)S(1)} %get-tuple-element.11, ...), kind=kOutput, calls=%fused_computation | convolution fusion | flops 727056384 | bytes 6717696 | tf_op jit(solution)/shard_map/dot_general | solution.py:41
  265.5 0.0 all-reduce.13.cloned.1.call-update
  265.5 59.4 %all-reduce.13.cloned.1.call-done = f32[256,1024]{1,0:T(8,128)} async-done(((f32[256,1024]{1,0:T(8,128)}), f32[256,1024]{1,0:T(8,128)}) %all-reduce.13.cloned.1.call-update) | async-done | bytes 1048592 | tf_op jit(solution)/shard_map/psum | solution.py:44
  324.9 2.2 fusion.43
  (2 shorter events, 0.0 us)
Async XLA Ops:
  6.5 93.1 %all-reduce.17.cloned.1.call-start = ((), (), s32[]{:S(2)}) async-start(), calls=%async_computation.3 | async-start | bytes 5636096 | tf_op jit(solution)/shard_map/psum | solution.py:36
  7.3 4.0 %copy-start = (bf16[256,1024]{1,0:T(8,128)(2,1)S(1)}, bf16[256,1024]{1,0:T(8,128)(2,1)}, u32[]{:S(2)}) copy-start(bf16[256,1024]{1,0:T(8,128)(2,1)} %param.7) | copy-start | bytes 1572868
  15.2 11.8 %copy-start.1 = (f32[2,3,1376]{2,0,1:T(2,128)S(1)}, f32[2,3,1376]{2,0,1:T(2,128)}, u32[]{:S(2)}) copy-start(f32[2,3,1376]{2,0,1:T(2,128)} %param.12) | copy-start | bytes 99076
  15.2 11.8 %copy-start.2 = (f32[2,3,1376]{2,0,1:T(2,128)S(1)}, f32[2,3,1376]{2,0,1:T(2,128)}, u32[]{:S(2)}) copy-start(f32[2,3,1376]{2,0,1:T(2,128)} %param.11) | copy-start | bytes 99076
  15.2 152.1 %all-reduce.11.cloned.1.call-start = ((), (), s32[]{:S(2)}) async-start(), calls=%async_computation | async-start | bytes 2097152 | tf_op jit(solution)/shard_map/psum | solution.py:44
  107.9 149.4 %all-reduce.15.cloned.1.call-start = ((), (), s32[]{:S(2)}) async-start(), calls=%async_computation.2 | async-start | bytes 5636096 | tf_op jit(solution)/shard_map/psum | solution.py:36
  176.5 148.4 %all-reduce.13.cloned.1.call-start = ((), (), s32[]{:S(2)}) async-start(), calls=%async_computation.1 | async-start | bytes 2097152 | tf_op jit(solution)/shard_map/psum | solution.py:44
Sparse Core Ops, SparseCore 0:
  15.3 84.2 all-reduce.16
  108.0 59.2 all-reduce.10
  176.6 80.6 all-reduce.14
  265.6 59.2 all-reduce.12
where the time goes:
time: 334 us
  waiting for transfers between devices  262 us (78%)
  matrix products  28 us (8%)
  blocking collectives  21.6 us (6%)
  between operations  13.2 us (4%)
  other arithmetic  7.81 us (2%)
    psum x2, waiting for transfers between devices, body(): gate_sum, value_sum = lax.psum((gate_part, value_part), 'ra')  143 us
    psum x2, waiting for transfers between devices, body(): branch = lax.psum(partial_branch, 'cb')  119 us
    psum x2, blocking collectives, body(): total_squares = lax.psum(local_squares, 'ra')  21.6 us
    dot_general x2, matrix products, body(): jnp.dot(hidden, down_weight[layer_index], preferred_element_type=jnp.floa...  12.5 us
    dot_general x2, matrix products, body(): jnp.dot(scaled, value_weight[layer_index], preferred_element_type=jnp.flo...  7.86 us
    dot_general x2, matrix products, body(): jnp.dot(scaled, gate_weight[layer_index], preferred_element_type=jnp.floa...  7.65 us
  transfers between devices with their start and end apart: 4, of which 4 were waited for; matrix products, arithmetic and copies ran while one was open for 0% of the time, Pallas kernels for 0%

commit v1 on v0

v1 whole, which is shorter than its diff:
```python
import functools

import jax
import jax.numpy as jnp
from jax import lax
from jax.experimental import pallas as pl
from jax.experimental.pallas import tpu as pltpu
from jax.sharding import PartitionSpec as P

epsilon = 1e-06
MESH = pl.DeviceIdType.MESH
CORES = 2


def lane_tiles(width, tile=512):
    return [(start, min(tile, width - start)) for start in range(0, width, tile)]


def schedule(layers, chunks):
    order = []
    for layer in range(layers):
        if chunks == 1:
            order += [(s, layer, 0) for s in ("ua", "ub", "h", "wa", "wb", "sa", "sb", "sc")]
            continue
        for c in range(chunks):
            order += [("sc", layer - 1, c)] if layer else []
            order += [("ua", layer, c), ("ub", layer, c)]
        for c in range(chunks):
            order += [("h", layer, c)]
            if c:
                order += [("wb", layer, c - 1)]
            order += [("wa", layer, c)]
            if c:
                order += [("sa", layer, c - 1)]
        order += [("wb", layer, chunks - 1)]
        for c in range(chunks - 1):
            order += [("sb", layer, c)]
        order += [("sa", layer, chunks - 1), ("sb", layer, chunks - 1)]
    if chunks > 1:
        order += [("sc", layers - 1, c) for c in range(chunks)]
    return order


def kernel(
    cfg,
    tokens, gain, gate_hbm, value_hbm, gate_taps, value_taps, down_hbm,
    out,
    wg, wv, wd, buf, sums_out, sums_in, part, part_in, hid, acc, half, half_in, red, red_in, strm,
    w_sem, sums_ss, sums_rs, part_ss, part_rs, hid_ss, hid_rs, half_ss, half_rs, red_ss, red_rs,
    strm_ss, strm_rs, pair_ss, pair_rs,
):
    layers, chunks, nr, nz, t, ff, d, total_d = cfg
    tr = t // nr
    tz = t // (CORES * nz)
    r = lax.axis_index("ra")
    cb = lax.axis_index("cb")
    z, k = cb // CORES, lax.rem(cb, CORES)
    pair = (r, z * CORES + 1 - k)

    def ra_peer(off):
        return lax.rem(r + off, nr)

    def z_peer(off):
        return lax.rem(z + off, nz)

    def weight_copies(layer):
        return [
            pltpu.make_async_copy(src.at[layer], dst.at[layer], w_sem.at[layer, i])
            for i, (src, dst) in enumerate(((gate_hbm, wg), (value_hbm, wv), (down_hbm, wd)))
        ]

    weights = [weight_copies(layer) for layer in range(layers)]
    for copies in weights:
        for copy in copies:
            copy.start()

    barrier = pltpu.get_barrier_semaphore()
    peers = [(ra_peer(o), cb) for o in range(1, nr)]
    peers += [(r, z_peer(o) * CORES + k) for o in range(1, nz)] + [pair]
    for peer in peers:
        pl.semaphore_signal(barrier, inc=1, device_id=peer, device_id_type=MESH)
    pl.semaphore_wait(barrier, len(peers))

    pending = []

    def send(src, dst, ssem, rsem, device):
        copy = pltpu.make_async_remote_copy(
            src_ref=src, dst_ref=dst, send_sem=ssem, recv_sem=rsem,
            device_id=device, device_id_type=MESH,
        )
        copy.start()
        pending.append(copy)

    def arrived(dst, ssem, rsem):
        pltpu.make_async_remote_copy(
            src_ref=dst, dst_ref=dst, send_sem=ssem, recv_sem=rsem,
            device_id=pair, device_id_type=MESH,
        ).wait_recv()

    def stream_of(layer, c):
        if layer == 0:
            return tokens[c * t:(c + 1) * t, :].astype(jnp.float32)
        return strm[layer - 1, c].astype(jnp.float32).reshape(t, d)

    def ua(layer, c):
        i = layer * chunks + c
        current = stream_of(layer, c)
        squares = current * current
        folded = squares[:, 0:128]
        for j in range(1, d // 128):
            folded = folded + squares[:, j * 128:(j + 1) * 128]
        row = jnp.sum(folded.T, axis=0, keepdims=True)
        sums_out[i] = jnp.broadcast_to(row, (8, t))
        for o in range(1, nr):
            send(sums_out.at[i], sums_in.at[i, o - 1], sums_ss.at[i, o - 1], sums_rs.at[i, o - 1],
                 (ra_peer(o), cb))
        scaled = (current * gain[layer:layer + 1, :]).astype(jnp.bfloat16)
        for g, w in ((0, wg), (1, wv)):
            if c == 0:
                weights[layer][g].wait()
                buf[g, 0:8, :] = jnp.zeros((8, ff), jnp.float32)
            else:
                buf[g, 0:8, :] = buf[g, t:t + 8, :]
            for start, size in lane_tiles(ff):
                buf[g, 8:8 + t, start:start + size] = jnp.dot(
                    scaled, w[layer, :, start:start + size], preferred_element_type=jnp.float32)

    def ub(layer, c):
        i = layer * chunks + c
        total = sums_out[i]
        for o in range(1, nr):
            arrived(sums_in.at[i, o - 1], sums_ss.at[i, o - 1], sums_rs.at[i, o - 1])
            total = total + sums_in[i, o - 1]
        inverse = lax.rsqrt(total / total_d + epsilon)
        inverse = jnp.broadcast_to(inverse[0:1, :], (128, t)).T[:, 0:1]
        for g, taps in ((0, gate_taps), (1, value_taps)):
            for start, size in lane_tiles(ff, 128):
                cols = slice(start, start + size)
                buf[g, 8:8 + t, cols] = buf[g, 8:8 + t, cols] * inverse
                width = taps.shape[1]
                result = None
                for offset in range(width):
                    first = 8 - (width - 1) + offset
                    term = taps[layer, offset:offset + 1, cols] * buf[g, first:first + t, cols]
                    result = term if result is None else result + term
                part[i, g, :, :, cols] = result.reshape(nr, tr, size).astype(jnp.bfloat16)
            for o in range(1, nr):
                send(part.at[i, g, ra_peer(o)], part_in.at[i, g, o - 1],
                     part_ss.at[i, g, o - 1], part_rs.at[i, g, o - 1], (ra_peer(o), cb))

    def h(layer, c):
        i = layer * chunks + c
        for g in range(2):
            for o in range(1, nr):
                arrived(part_in.at[i, g, o - 1], part_ss.at[i, g, o - 1], part_rs.at[i, g, o - 1])
        pair_of = []
        for g in range(2):
            total = part[i, g, r].astype(jnp.float32)
            for o in range(1, nr):
                total = total + part_in[i, g, o - 1].astype(jnp.float32)
            pair_of.append(total)
        gate, value = pair_of
        hid[i, r] = (jax.nn.silu(gate) * value).astype(jnp.bfloat16)
        for o in range(1, nr):
            send(hid.at[i, r], hid.at[i, r], hid_ss.at[i, o - 1], hid_rs.at[i, o - 1],
                 (ra_peer(o), cb))

    def wa(layer, c):
        i = layer * chunks + c
        for o in range(1, nr):
            arrived(hid.at[i, ra_peer(nr - o)], hid_ss.at[i, o - 1], hid_rs.at[i, o - 1])
        if c == 0:
            weights[layer][2].wait()
        hidden = hid[i].reshape(t, ff)
        for start, size in lane_tiles(d):
            branch = jnp.dot(hidden, wd[layer, :, start:start + size],
                             preferred_element_type=jnp.float32)
            acc[c, :, :, start:start + size] = branch.reshape(CORES, t // CORES, size)
        half[i] = acc[c, 1 - k].astype(jnp.bfloat16)
        send(half.at[i], half_in.at[i], half_ss.at[i], half_rs.at[i], pair)

    def wb(layer, c):
        i = layer * chunks + c
        arrived(half_in.at[i], half_ss.at[i], half_rs.at[i])
        total = acc[c, k] + half_in[i].astype(jnp.float32)
        acc[c, k] = total
        red[i] = total.reshape(nz, tz, d).astype(jnp.bfloat16)
        for o in range(1, nz):
            send(red.at[i, z_peer(o)], red_in.at[i, o - 1], red_ss.at[i, o - 1], red_rs.at[i, o - 1],
                 (r, z_peer(o) * CORES + k))

    def sa(layer, c):
        i = layer * chunks + c
        if layer == 0:
            first = c * t + (k * nz + z) * tz
            current = tokens[pl.ds(pl.multiple_of(first, tz), tz), :].astype(jnp.float32)
        else:
            current = strm[layer - 1, c, k, z].astype(jnp.float32)
        total = red[i, z].astype(jnp.float32)
        for o in range(1, nz):
            arrived(red_in.at[i, o - 1], red_ss.at[i, o - 1], red_rs.at[i, o - 1])
            total = total + red_in[i, o - 1].astype(jnp.float32)
        strm[layer, c, k, z] = (0.5 * current + total).astype(jnp.bfloat16)
        for o in range(1, nz):
            mine = strm.at[layer, c, k, z]
            send(mine, mine, strm_ss.at[i, o - 1], strm_rs.at[i, o - 1],
                 (r, z_peer(o) * CORES + k))

    def sb(layer, c):
        i = layer * chunks + c
        for o in range(1, nz):
            arrived(strm.at[layer, c, k, z_peer(nz - o)], strm_ss.at[i, o - 1], strm_rs.at[i, o - 1])
        mine = strm.at[layer, c, k]
        send(mine, mine, pair_ss.at[i], pair_rs.at[i], pair)

    def sc(layer, c):
        i = layer * chunks + c
        arrived(strm.at[layer, c, 1 - k], pair_ss.at[i], pair_rs.at[i])
        if layer == layers - 1:
            final = strm[layer, c].astype(jnp.float32).reshape(t, d)
            out[c * t:(c + 1) * t, :] = final.astype(jnp.bfloat16)

    steps = dict(ua=ua, ub=ub, h=h, wa=wa, wb=wb, sa=sa, sb=sb, sc=sc)
    for name, layer, c in schedule(layers, chunks):
        steps[name](layer, c)
    for copy in pending:
        copy.wait_send()


def body(nr, nc, tokens, norm_gain, gate_weight, value_weight, gate_taps, value_taps, down_weight):
    layers, d, ff = gate_weight.shape
    rows = tokens.shape[0]
    nz = nc // CORES
    chunks = 2 if rows // 2 >= 16 * max(nr, nc) else 1
    t = rows // chunks
    n = layers * chunks
    cfg = (layers, chunks, nr, nz, t, ff, d, d * nr)
    bf16, f32 = jnp.bfloat16, jnp.float32
    dma = pltpu.SemaphoreType.DMA
    vmem = pl.BlockSpec(memory_space=pltpu.VMEM)
    hbm = pl.BlockSpec(memory_space=pltpu.HBM)
    tz = t // nc
    return pl.pallas_call(
        functools.partial(kernel, cfg),
        out_shape=jax.ShapeDtypeStruct((rows, d), bf16),
        in_specs=[vmem, vmem, hbm, hbm, vmem, vmem, hbm],
        out_specs=vmem,
        scratch_shapes=[
            pltpu.VMEM((layers, d, ff), bf16),
            pltpu.VMEM((layers, d, ff), bf16),
            pltpu.VMEM((layers, ff, d), bf16),
            pltpu.VMEM((2, 8 + t, ff), f32),
            pltpu.VMEM((n, 8, t), f32),
            pltpu.VMEM((n, nr - 1, 8, t), f32),
            pltpu.VMEM((n, 2, nr, t // nr, ff), bf16),
            pltpu.VMEM((n, 2, nr - 1, t // nr, ff), bf16),
            pltpu.VMEM((n, nr, t // nr, ff), bf16),
            pltpu.VMEM((chunks, CORES, t // CORES, d), f32),
            pltpu.VMEM((n, t // CORES, d), bf16),
            pltpu.VMEM((n, t // CORES, d), bf16),
            pltpu.VMEM((n, nz, tz, d), bf16),
            pltpu.VMEM((n, nz - 1, tz, d), bf16),
            pltpu.VMEM((layers, chunks, CORES, nz, tz, d), bf16),
            dma((layers, 3)),
            dma((n, nr - 1)), dma((n, nr - 1)),
            dma((n, 2, nr - 1)), dma((n, 2, nr - 1)),
            dma((n, nr - 1)), dma((n, nr - 1)),
            dma((n,)), dma((n,)),
            dma((n, nz - 1)), dma((n, nz - 1)),
            dma((n, nz - 1)), dma((n, nz - 1)),
            dma((n,)), dma((n,)),
        ],
        compiler_params=pltpu.CompilerParams(
            collective_id=0, has_side_effects=True, vmem_limit_bytes=60 * 1024 * 1024,
        ),
    )(tokens, norm_gain, gate_weight, value_weight, gate_taps, value_taps, down_weight)


def solution(mesh):
    return jax.shard_map(
        functools.partial(body, mesh.shape["ra"], mesh.shape["cb"]),
        mesh=mesh,
        in_specs=(
            P(None, "ra"),
            P(None, "ra"),
            P(None, "ra", "cb"),
            P(None, "ra", "cb"),
            P(None, None, "cb"),
            P(None, None, "cb"),
            P(None, "cb", "ra"),
        ),
        out_specs=P(None, "ra"),
        check_vma=False,
    )
```

time: 334 us -> 118 us (0.35)
  waiting for transfers between devices: 262 us -> 0 us
  Pallas kernels: 0 us -> 95.6 us
  matrix products: 28 us -> 0 us
  blocking collectives: 21.6 us -> 0 us
  local copies, waits for them, and re-layouts: 0.97 us -> 21.4 us
  between operations: 13.2 us -> 0.01 us
  other arithmetic: 7.81 us -> 0 us
    psum x4 -> x0, waiting for transfers between devices: 262 us -> none  [the longest x2 143 us: body(): gate_sum, value_sum = lax.psum((gate_part, value_part), 'ra')]
    pallas_call x0 -> x1, Pallas kernels: none -> 95.6 us  [body(): pl.pallas_call(functools.partial(kernel, cfg), out_shape=jax.ShapeDtypeSt...]
    dot_general x6 -> x0, matrix products: 28 us -> none  [the longest x2 12.5 us: body(): jnp.dot(hidden, down_weight[layer_index], preferred_element_type=jnp.floa...]
    psum x2 -> x0, blocking collectives: 21.6 us -> none  [body(): total_squares = lax.psum(local_squares, 'ra')]
    unnamed x6 -> x5, local copies, waits for them, and re-layouts: 0.01 us -> 21.4 us
    mul x2 -> x0, other arithmetic: 3.92 us -> none  [body(): gate_conv = causal_conv(gate_sum * inverse_rms, gate_taps[layer_index])]
  transfers between devices with their start and end apart: 4 -> 0, of which waited for: 4 -> 0; matrix products, arithmetic and copies ran while one was open for 0% -> 0% of each run, Pallas kernels for 0% -> 0%
where the time goes in v1:
time: 118 us; the launch traced here: 117 us
  Pallas kernels  95.6 us (81%)
  local copies, waits for them, and re-layouts  21.4 us (18%)
    pallas_call x1, Pallas kernels, body(): pl.pallas_call(functools.partial(kernel, cfg), out_shape=jax.ShapeDtypeSt...  95.6 us
    unnamed x5, local copies, waits for them, and re-layouts  21.4 us

profile of v1, /device:TPU:0, one launch (start us, length us, event | category | flops | bytes accessed | tf_op | source)
XLA Modules:
  0.0 117.0 jit_solution(11032729540281793570)
XLA Ops:
  0.0 1.4 %copy.10.gate_taps = f32[2,3,1376]{2,1,0:T(4,128)} copy(f32[2,3,1376]{2,0,1:T(2,128)} %param.11) | data formatting | bytes 66048 | tf_op args[4]
  1.4 1.4 %copy.11.value_taps = f32[2,3,1376]{2,1,0:T(4,128)} copy(f32[2,3,1376]{2,0,1:T(2,128)} %param.12) | data formatting | bytes 66048 | tf_op args[5]
  2.8 8.4 %copy.8.gate_hbm = bf16[2,1024,1376]{2,1,0:T(8,128)(2,1)} copy(bf16[2,1024,1376]{1,2,0:T(8,128)(2,1)} %param.9) | data formatting | bytes 11272192 | tf_op args[2]
  11.1 8.4 %copy.9.value_hbm = bf16[2,1024,1376]{2,1,0:T(8,128)(2,1)} copy(bf16[2,1024,1376]{1,2,0:T(8,128)(2,1)} %param.10) | data formatting | bytes 11272192 | tf_op args[3]
  19.5 95.6 %shard_map.73 = bf16[256,1024]{1,0:T(8,128)(2,1)} custom-call(bf16[256,1024]{1,0:T(8,128)(2,1)} %tokens.1, f32[2,1024]{1,0:T(2,128)} %gain.1, bf16[2,1024,1376]{2,1,0:T(8,128)(2,1)} %copy.8.gate_hbm, bf16[2,1024,1376]{2,1,0:T(8,128)(2,1)} %copy.9.value_hbm, f32[2,3,1376]{2,1,0:T(4,128)} %copy.10.gate_taps, f32[2,3,1376]{2,1,0:T(4,128)} %copy.11.value_taps, ...), custom_call_target="tpu_custom_call" | custom-call | tf_op jit(solution)/shard_map/pallas_call | solution.py:243
  115.1 1.9 %copy.13 = bf16[256,1024]{1,0:T(8,128)(2,1)} copy(bf16[256,1024]{1,0:T(8,128)(2,1)} %shard_map.73) | data formatting | bytes 1048576

commit v2 on v1

--- a/solution.py
+++ b/solution.py
@@ -16,46 +16,50 @@
     return [(start, min(tile, width - start)) for start in range(0, width, tile)]
 
 
+STAGES = dict(u=0.0, x2=7.0, h=10.5, g2=14.0, wa=17.0, wb=19.5, sa=24.0, sb=28.5, sc=30.0)
+LAYER_TIME = 32.0
+CHUNK_TIME = 4.0
+
+
 def schedule(layers, chunks):
-    order = []
-    for layer in range(layers):
-        if chunks == 1:
-            order += [(s, layer, 0) for s in ("ua", "ub", "h", "wa", "wb", "sa", "sb", "sc")]
-            continue
-        for c in range(chunks):
-            order += [("sc", layer - 1, c)] if layer else []
-            order += [("ua", layer, c), ("ub", layer, c)]
-        for c in range(chunks):
-            order += [("h", layer, c)]
-            if c:
-                order += [("wb", layer, c - 1)]
-            order += [("wa", layer, c)]
-            if c:
-                order += [("sa", layer, c - 1)]
-        order += [("wb", layer, chunks - 1)]
-        for c in range(chunks - 1):
-            order += [("sb", layer, c)]
-        order += [("sa", layer, chunks - 1), ("sb", layer, chunks - 1)]
-    if chunks > 1:
-        order += [("sc", layers - 1, c) for c in range(chunks)]
-    return order
+    steps = [
+        (layer * LAYER_TIME + c * CHUNK_TIME + when, layer, c, name)
+        for layer in range(layers) for c in range(chunks) for name, when in STAGES.items()
+    ]
+    return [(name, layer, c) for _, layer, c, name in sorted(steps)]
 
 
 def kernel(
     cfg,
     tokens, gain, gate_hbm, value_hbm, gate_taps, value_taps, down_hbm,
     out,
-    wg, wv, wd, buf, sums_out, sums_in, part, part_in, hid, acc, half, half_in, red, red_in, strm,
-    w_sem, sums_ss, sums_rs, part_ss, part_rs, hid_ss, hid_rs, half_ss, half_rs, red_ss, red_rs,
-    strm_ss, strm_rs, pair_ss, pair_rs,
+    wg, wv, wd, buf, sums_out, sums_in, part, gate_one, value_one, mid, gate_two, value_two,
+    hid, acc, half, half_in, red, red_in, strm,
+    w_sem, sums_ss, sums_rs, g1_ss, g1_rs, v1_ss, v1_rs, g2_ss, g2_rs, v2_ss, v2_rs,
+    ax1_ss, ax1_rs, ay1_ss, ay1_rs, ax2_ss, ax2_rs, ay2_ss, ay2_rs,
+    half_ss, half_rs, red_ss, red_rs, strm_ss, strm_rs, pair_ss, pair_rs,
 ):
-    layers, chunks, nr, nz, t, ff, d, total_d = cfg
+    layers, chunks, ny, nx, nz, t, ff, d, total_d = cfg
+    nr = ny * nx
     tr = t // nr
     tz = t // (CORES * nz)
     r = lax.axis_index("ra")
     cb = lax.axis_index("cb")
     z, k = cb // CORES, lax.rem(cb, CORES)
     pair = (r, z * CORES + 1 - k)
+    y, x = r // nx, lax.rem(r, nx)
+
+    def y_peer(off):
+        return lax.rem(y + off, ny)
+
+    def x_peer(off):
+        return lax.rem(x + off, nx)
+
+    def at_y(row):
+        return (row * nx + x, cb)
+
+    def at_x(column):
+        return (y * nx + column, cb)
 
     def ra_peer(off):
         return lax.rem(r + off, nr)
@@ -101,6 +105,10 @@
         if layer == 0:
             return tokens[c * t:(c + 1) * t, :].astype(jnp.float32)
         return strm[layer - 1, c].astype(jnp.float32).reshape(t, d)
+
+    def u(layer, c):
+        ua(layer, c)
+        ub(layer, c)
 
     def ua(layer, c):
         i = layer * chunks + c
@@ -118,12 +126,13 @@
         for g, w in ((0, wg), (1, wv)):
             if c == 0:
                 weights[layer][g].wait()
-                buf[g, 0:8, :] = jnp.zeros((8, ff), jnp.float32)
+                buf[layer, g, 0:8, :] = jnp.zeros((8, ff), jnp.float32)
             else:
-                buf[g, 0:8, :] = buf[g, t:t + 8, :]
+                buf[layer, g, 0:8, :] = buf[layer, g, t:t + 8, :]
             for start, size in lane_tiles(ff):
-                buf[g, 8:8 + t, start:start + size] = jnp.dot(
-                    scaled, w[layer, :, start:start + size], preferred_element_type=jnp.float32)
+                buf[layer, g, 8:8 + t, start:start + size] = lax.dot_general(
+                    scaled, w[layer, start:start + size, :], (((1,), (1,)), ((), ())),
+                    preferred_element_type=jnp.float32)
 
     def ub(layer, c):
         i = layer * chunks + c
@@ -136,39 +145,88 @@
         for g, taps in ((0, gate_taps), (1, value_taps)):
             for start, size in lane_tiles(ff, 128):
                 cols = slice(start, start + size)
-                buf[g, 8:8 + t, cols] = buf[g, 8:8 + t, cols] * inverse
-                width = taps.shape[1]
+                buf[layer, g, 8:8 + t, cols] = buf[layer, g, 8:8 + t, cols] * inverse
+                width = taps.shape[0]
                 result = None
                 for offset in range(width):
                     first = 8 - (width - 1) + offset
-                    term = taps[layer, offset:offset + 1, cols] * buf[g, first:first + t, cols]
+                    term = taps[offset, layer:layer + 1, cols] * buf[layer, g, first:first + t, cols]
                     result = term if result is None else result + term
-                part[i, g, :, :, cols] = result.reshape(nr, tr, size).astype(jnp.bfloat16)
-            for o in range(1, nr):
-                send(part.at[i, g, ra_peer(o)], part_in.at[i, g, o - 1],
-                     part_ss.at[i, g, o - 1], part_rs.at[i, g, o - 1], (ra_peer(o), cb))
+                part[i, g, :, :, :, cols] = result.reshape(ny, nx, tr, size).astype(jnp.bfloat16)
+            if g == 0:
+                for o in range(1, nx):
+                    send(part.at[i, 0, :, x_peer(o)], gate_one.at[i, o - 1],
+                         g1_ss.at[i, o - 1], g1_rs.at[i, o - 1], at_x(x_peer(o)))
+            else:
+                for o in range(1, ny):
+                    send(part.at[i, 1, y_peer(o)], value_one.at[i, o - 1],
+                         v1_ss.at[i, o - 1], v1_rs.at[i, o - 1], at_y(y_peer(o)))
+
+    def gate_sum(i, row):
+        total = part[i, 0, row, x].astype(jnp.float32)
+        for o in range(1, nx):
+            total = total + gate_one[i, o - 1, row].astype(jnp.float32)
+        return total
+
+    def value_sum(i, column):
+        total = part[i, 1, y, column].astype(jnp.float32)
+        for o in range(1, ny):
+            total = total + value_one[i, o - 1, column].astype(jnp.float32)
+        return total
+
+    def x2(layer, c):
+        i = layer * chunks + c
+        for o in range(1, nx):
+            arrived(gate_one.at[i, o - 1], g1_ss.at[i, o - 1], g1_rs.at[i, o - 1])
+        for o in range(1, ny):
+            mid[i, 0, o - 1] = gate_sum(i, y_peer(o)).astype(jnp.bfloat16)
+            send(mid.at[i, 0, o - 1], gate_two.at[i, o - 1],
+                 g2_ss.at[i, o - 1], g2_rs.at[i, o - 1], at_y(y_peer(o)))
+        for o in range(1, ny):
+            arrived(value_one.at[i, o - 1], v1_ss.at[i, o - 1], v1_rs.at[i, o - 1])
+        for o in range(1, nx):
+            mid[i, 1, o - 1] = value_sum(i, x_peer(o)).astype(jnp.bfloat16)
+            send(mid.at[i, 1, o - 1], value_two.at[i, o - 1],
+                 v2_ss.at[i, o - 1], v2_rs.at[i, o - 1], at_x(x_peer(o)))
 
     def h(layer, c):
         i = layer * chunks + c
-        for g in range(2):
-            for o in range(1, nr):
-                arrived(part_in.at[i, g, o - 1], part_ss.at[i, g, o - 1], part_rs.at[i, g, o - 1])
-        pair_of = []
-        for g in range(2):
-            total = part[i, g, r].astype(jnp.float32)
-            for o in range(1, nr):
-                total = total + part_in[i, g, o - 1].astype(jnp.float32)
-            pair_of.append(total)
-        gate, value = pair_of
-        hid[i, r] = (jax.nn.silu(gate) * value).astype(jnp.bfloat16)
-        for o in range(1, nr):
-            send(hid.at[i, r], hid.at[i, r], hid_ss.at[i, o - 1], hid_rs.at[i, o - 1],
-                 (ra_peer(o), cb))
+        gate = gate_sum(i, y)
+        for o in range(1, ny):
+            arrived(gate_two.at[i, o - 1], g2_ss.at[i, o - 1], g2_rs.at[i, o - 1])
+            gate = gate + gate_two[i, o - 1].astype(jnp.float32)
+        value = value_sum(i, x)
+        for o in range(1, nx):
+            arrived(value_two.at[i, o - 1], v2_ss.at[i, o - 1], v2_rs.at[i, o - 1])
+            value = value + value_two[i, o - 1].astype(jnp.float32)
+        hidden = (jax.nn.silu(gate) * value).reshape(2, tr // 2, ff)
+        hid[i, y, x] = hidden.astype(jnp.bfloat16)
+        for o in range(1, nx):
+            mine = hid.at[i, y, x, 0]
+            send(mine, mine, ax1_ss.at[i, o - 1], ax1_rs.at[i, o - 1], at_x(x_peer(o)))
+        for o in range(1, ny):
+            mine = hid.at[i, y, x, 1]
+            send(mine, mine, ay1_ss.at[i, o - 1], ay1_rs.at[i, o - 1], at_y(y_peer(o)))
+
+    def g2(layer, c):
+        i = layer * chunks + c
+        for o in range(1, nx):
+            arrived(hid.at[i, y, x_peer(nx - o), 0], ax1_ss.at[i, o - 1], ax1_rs.at[i, o - 1])
+        for o in range(1, ny):
+            mine = hid.at[i, y, :, 0]
+            send(mine, mine, ay2_ss.at[i, o - 1], ay2_rs.at[i, o - 1], at_y(y_peer(o)))
+        for o in range(1, ny):
+            arrived(hid.at[i, y_peer(ny - o), x, 1], ay1_ss.at[i, o - 1], ay1_rs.at[i, o - 1])
+        for o in range(1, nx):
+            mine = hid.at[i, :, x, 1]
+            send(mine, mine, ax2_ss.at[i, o - 1], ax2_rs.at[i, o - 1], at_x(x_peer(o)))
 
     def wa(layer, c):
         i = layer * chunks + c
-        for o in range(1, nr):
-            arrived(hid.at[i, ra_peer(nr - o)], hid_ss.at[i, o - 1], hid_rs.at[i, o - 1])
+        for o in range(1, ny):
+            arrived(hid.at[i, y_peer(ny - o), :, 0], ay2_ss.at[i, o - 1], ay2_rs.at[i, o - 1])
+        for o in range(1, nx):
+            arrived(hid.at[i, :, x_peer(nx - o), 1], ax2_ss.at[i, o - 1], ax2_rs.at[i, o - 1])
         if c == 0:
             weights[layer][2].wait()
         hidden = hid[i].reshape(t, ff)
@@ -220,7 +278,7 @@
             final = strm[layer, c].astype(jnp.float32).reshape(t, d)
             out[c * t:(c + 1) * t, :] = final.astype(jnp.bfloat16)
 
-    steps = dict(ua=ua, ub=ub, h=h, wa=wa, wb=wb, sa=sa, sb=sb, sc=sc)
+    steps = dict(u=u, x2=x2, h=h, g2=g2, wa=wa, wb=wb, sa=sa, sb=sb, sc=sc)
     for name, layer, c in schedule(layers, chunks):
         steps[name](layer, c)
     for copy in pending:
@@ -229,32 +287,41 @@
 
 def body(nr, nc, tokens, norm_gain, gate_weight, value_weight, gate_taps, value_taps, down_weight):
     layers, d, ff = gate_weight.shape
+    gate_weight, value_weight = (jnp.swapaxes(w, 1, 2) for w in (gate_weight, value_weight))
+    gate_taps, value_taps = (jnp.swapaxes(w, 0, 1) for w in (gate_taps, value_taps))
+    ny = max(f for f in range(1, nr + 1) if nr % f == 0 and f * f <= nr)
+    nx = nr // ny
     rows = tokens.shape[0]
     nz = nc // CORES
     chunks = 2 if rows // 2 >= 16 * max(nr, nc) else 1
     t = rows // chunks
     n = layers * chunks
-    cfg = (layers, chunks, nr, nz, t, ff, d, d * nr)
+    cfg = (layers, chunks, ny, nx, nz, t, ff, d, d * nr)
     bf16, f32 = jnp.bfloat16, jnp.float32
     dma = pltpu.SemaphoreType.DMA
     vmem = pl.BlockSpec(memory_space=pltpu.VMEM)
     hbm = pl.BlockSpec(memory_space=pltpu.HBM)
-    tz = t // nc
+    tz, tr = t // nc, t // nr
+    px, py = max(nx - 1, 1), max(ny - 1, 1)
     return pl.pallas_call(
         functools.partial(kernel, cfg),
         out_shape=jax.ShapeDtypeStruct((rows, d), bf16),
         in_specs=[vmem, vmem, hbm, hbm, vmem, vmem, hbm],
         out_specs=vmem,
         scratch_shapes=[
-            pltpu.VMEM((layers, d, ff), bf16),
-            pltpu.VMEM((layers, d, ff), bf16),
             pltpu.VMEM((layers, ff, d), bf16),
-            pltpu.VMEM((2, 8 + t, ff), f32),
+            pltpu.VMEM((layers, ff, d), bf16),
+            pltpu.VMEM((layers, ff, d), bf16),
+            pltpu.VMEM((layers, 2, 8 + t, ff), f32),
             pltpu.VMEM((n, 8, t), f32),
             pltpu.VMEM((n, nr - 1, 8, t), f32),
-            pltpu.VMEM((n, 2, nr, t // nr, ff), bf16),
-            pltpu.VMEM((n, 2, nr - 1, t // nr, ff), bf16),
-            pltpu.VMEM((n, nr, t // nr, ff), bf16),
+            pltpu.VMEM((n, 2, ny, nx, tr, ff), bf16),
+            pltpu.VMEM((n, px, ny, tr, ff), bf16),
+            pltpu.VMEM((n, py, nx, tr, ff), bf16),
+            pltpu.VMEM((n, 2, max(px, py), tr, ff), bf16),
+            pltpu.VMEM((n, py, tr, ff), bf16),
+            pltpu.VMEM((n, px, tr, ff), bf16),
+            pltpu.VMEM((n, ny, nx, 2, tr // 2, ff), bf16),
             pltpu.VMEM((chunks, CORES, t // CORES, d), f32),
             pltpu.VMEM((n, t // CORES, d), bf16),
             pltpu.VMEM((n, t // CORES, d), bf16),
@@ -263,8 +330,10 @@
             pltpu.VMEM((layers, chunks, CORES, nz, tz, d), bf16),
             dma((layers, 3)),
             dma((n, nr - 1)), dma((n, nr - 1)),
-            dma((n, 2, nr - 1)), dma((n, 2, nr - 1)),
-            dma((n, nr - 1)), dma((n, nr - 1)),
+            dma((n, px)), dma((n, px)), dma((n, py)), dma((n, py)),
+            dma((n, py)), dma((n, py)), dma((n, px)), dma((n, px)),
+            dma((n, px)), dma((n, px)), dma((n, py)), dma((n, py)),
+            dma((n, px)), dma((n, px)), dma((n, py)), dma((n, py)),
             dma((n,)), dma((n,)),
             dma((n, nz - 1)), dma((n, nz - 1)),
             dma((n, nz - 1)), dma((n, nz - 1)),

time: 118 us -> 91.2 us (0.77)
  local copies, waits for them, and re-layouts: 21.4 us -> 1.87 us
  Pallas kernels: 95.6 us -> 89.2 us
    unnamed x5 -> x1, local copies, waits for them, and re-layouts: 21.4 us -> 1.87 us
    pallas_call x1, Pallas kernels: 95.6 us -> 89.2 us  [body(): pl.pallas_call(functools.partial(kernel, cfg), out_shape=jax.ShapeDtypeSt...]
where the time goes in v2:
time: 91.2 us; the launch traced here: 91 us
  Pallas kernels  89.2 us (98%)
  local copies, waits for them, and re-layouts  1.87 us (2%)
    pallas_call x1, Pallas kernels, body(): pl.pallas_call(functools.partial(kernel, cfg), out_shape=jax.ShapeDtypeSt...  89.2 us
    unnamed x1, local copies, waits for them, and re-layouts  1.87 us

profile of v2, /device:TPU:0, one launch (start us, length us, event | category | flops | bytes accessed | tf_op | source)
XLA Modules:
  0.0 91.0 jit_solution(14080988186840548736)
XLA Ops:
  0.0 89.2 %shard_map.73 = bf16[256,1024]{1,0:T(8,128)(2,1)} custom-call(bf16[256,1024]{1,0:T(8,128)(2,1)} %tokens.1, f32[2,1024]{1,0:T(2,128)} %gain.1, bf16[2,1376,1024]{2,1,0:T(8,128)(2,1)} %bitcast.4, bf16[2,1376,1024]{2,1,0:T(8,128)(2,1)} %bitcast.5, f32[3,2,1376]{2,1,0:T(2,128)} %bitcast.6, f32[3,2,1376]{2,1,0:T(2,128)} %bitcast.7, bf16[2,1376,1024]{2,1,0:T(8,128)(2,1)} %down_hbm.1), custom_call_target="tpu_custom_call" | custom-call | tf_op jit(solution)/shard_map/pallas_call | solution.py:306
  89.2 1.9 %copy.9 = bf16[256,1024]{1,0:T(8,128)(2,1)} copy(bf16[256,1024]{1,0:T(8,128)(2,1)} %shard_map.73) | data formatting | bytes 1048576

commit v3 on v2

--- a/solution.py
+++ b/solution.py
@@ -10,30 +10,69 @@
 epsilon = 1e-06
 MESH = pl.DeviceIdType.MESH
 CORES = 2
+LANES = 128
 
 
 def lane_tiles(width, tile=512):
     return [(start, min(tile, width - start)) for start in range(0, width, tile)]
 
 
-STAGES = dict(u=0.0, x2=7.0, h=10.5, g2=14.0, wa=17.0, wb=19.5, sa=24.0, sb=28.5, sc=30.0)
-LAYER_TIME = 32.0
-CHUNK_TIME = 4.0
-
-
-def schedule(layers, chunks):
-    steps = [
-        (layer * LAYER_TIME + c * CHUNK_TIME + when, layer, c, name)
-        for layer in range(layers) for c in range(chunks) for name, when in STAGES.items()
-    ]
-    return [(name, layer, c) for _, layer, c, name in sorted(steps)]
+LINK_RATE = 46000.0
+PAIR_RATE = 300000.0
+LATENCY = 2.0
+STAGGER = 0.0
+PAIR_LATENCY = 1.1
+WORK = dict(s=0.2, u=2.0, x2=0.5, h=0.5, g2=0.1, wa=0.7, wb=0.2, sa=0.2, sb=0.1, sc=0.1)
+
+
+def schedule(layers, chunks, ny, nx, nz, t, ff, d):
+    nr = ny * nx
+    third = max(1.0, (nz * nz) / 4.0)
+    up = 2.0 * t * ff / nr
+    down = 2.0 * t * d / (CORES * nz)
+    sends = dict(
+        s=dict(x=100.0, y=100.0),
+        u=dict(x=up * ny * (nx - 1), y=up * nx * (ny - 1)),
+        x2=dict(y=up * (ny - 1), x=up * (nx - 1)),
+        h=dict(x=up / 2 * (nx - 1), y=up / 2 * (ny - 1)),
+        g2=dict(x=up / 2 * ny * (nx - 1), y=up / 2 * nx * (ny - 1)),
+        wa=dict(p=down * nz),
+        wb=dict(z=down * third),
+        sa=dict(z=down * third),
+        sb=dict(p=down * nz),
+        sc=dict(),
+    )
+    names = list(sends)
+    free = dict(x=0.0, y=0.0, z=0.0, p=0.0)
+    ready = {c: c * STAGGER for c in range(chunks)}
+    place = {c: 0 for c in range(chunks)}
+    now, order, depth = 0.0, [], len(names)
+    while len(order) < layers * chunks * depth:
+        open_chunks = []
+        for c in range(chunks):
+            if place[c] == layers * depth:
+                continue
+            if names[place[c] % depth] == "u" and c and place[c - 1] <= place[c]:
+                continue
+            open_chunks.append((max(ready[c], now), c))
+        when, c = min(open_chunks)
+        name = names[place[c] % depth]
+        order.append((name, place[c] // depth, c))
+        place[c] += 1
+        now = when + WORK[name] * t / 128
+        ready[c] = now
+        for link, size in sends[name].items():
+            rate, lag = (PAIR_RATE, PAIR_LATENCY) if link == "p" else (LINK_RATE, LATENCY)
+            free[link] = max(free[link], now) + size / rate
+            ready[c] = max(ready[c], free[link] + lag)
+    return order
 
 
 def kernel(
     cfg,
     tokens, gain, gate_hbm, value_hbm, gate_taps, value_taps, down_hbm,
     out,
-    wg, wv, wd, buf, sums_out, sums_in, part, gate_one, value_one, mid, gate_two, value_two,
+    wg, wv, wd, turned, buf, sums_out, sums_in, part, gate_one, value_one, mid, gate_two, value_two,
     hid, acc, half, half_in, red, red_in, strm,
     w_sem, sums_ss, sums_rs, g1_ss, g1_rs, v1_ss, v1_rs, g2_ss, g2_rs, v2_ss, v2_rs,
     ax1_ss, ax1_rs, ay1_ss, ay1_rs, ax2_ss, ax2_rs, ay2_ss, ay2_rs,
@@ -74,9 +113,8 @@
         ]
 
     weights = [weight_copies(layer) for layer in range(layers)]
-    for copies in weights:
-        for copy in copies:
-            copy.start()
+    for copy in weights[0][:2]:
+        copy.start()
 
     barrier = pltpu.get_barrier_semaphore()
     peers = [(ra_peer(o), cb) for o in range(1, nr)]
@@ -106,11 +144,7 @@
             return tokens[c * t:(c + 1) * t, :].astype(jnp.float32)
         return strm[layer - 1, c].astype(jnp.float32).reshape(t, d)
 
-    def u(layer, c):
-        ua(layer, c)
-        ub(layer, c)
-
-    def ua(layer, c):
+    def s(layer, c):
         i = layer * chunks + c
         current = stream_of(layer, c)
         squares = current * current
@@ -122,20 +156,37 @@
         for o in range(1, nr):
             send(sums_out.at[i], sums_in.at[i, o - 1], sums_ss.at[i, o - 1], sums_rs.at[i, o - 1],
                  (ra_peer(o), cb))
+
+    def turn(layer):
+        for g, w in ((0, wg), (1, wv)):
+            weights[layer][g].wait()
+            for start, size in lane_tiles(ff, 128):
+                turned[layer - 1, g, :, start:start + size] = w[layer, start:start + size, :].T
+
+    def u(layer, c):
+        i = layer * chunks + c
+        current = stream_of(layer, c)
         scaled = (current * gain[layer:layer + 1, :]).astype(jnp.bfloat16)
         for g, w in ((0, wg), (1, wv)):
             if c == 0:
-                weights[layer][g].wait()
+                if layer == 0:
+                    weights[layer][g].wait()
+                    later = [weights[0][2]] if g == 0 else [w for ws in weights[1:] for w in ws]
+                    for copy in later:
+                        copy.start()
                 buf[layer, g, 0:8, :] = jnp.zeros((8, ff), jnp.float32)
             else:
                 buf[layer, g, 0:8, :] = buf[layer, g, t:t + 8, :]
             for start, size in lane_tiles(ff):
-                buf[layer, g, 8:8 + t, start:start + size] = lax.dot_general(
-                    scaled, w[layer, start:start + size, :], (((1,), (1,)), ((), ())),
-                    preferred_element_type=jnp.float32)
-
-    def ub(layer, c):
-        i = layer * chunks + c
+                if layer:
+                    product = jnp.dot(scaled, turned[layer - 1, g, :, start:start + size],
+                                      preferred_element_type=jnp.float32)
+                else:
+                    product = lax.dot_general(
+                        scaled, w[layer, start:start + size, :], (((1,), (1,)), ((), ())),
+                        preferred_element_type=jnp.float32)
+                buf[layer, g, 8:8 + t, start:start + size] = product
+
         total = sums_out[i]
         for o in range(1, nr):
             arrived(sums_in.at[i, o - 1], sums_ss.at[i, o - 1], sums_rs.at[i, o - 1])
@@ -199,7 +250,7 @@
         for o in range(1, nx):
             arrived(value_two.at[i, o - 1], v2_ss.at[i, o - 1], v2_rs.at[i, o - 1])
             value = value + value_two[i, o - 1].astype(jnp.float32)
-        hidden = (jax.nn.silu(gate) * value).reshape(2, tr // 2, ff)
+        hidden = (jax.nn.silu(gate) * value).reshape(2, tr // 2, -1)
         hid[i, y, x] = hidden.astype(jnp.bfloat16)
         for o in range(1, nx):
             mine = hid.at[i, y, x, 0]
@@ -229,7 +280,7 @@
             arrived(hid.at[i, :, x_peer(nx - o), 1], ax2_ss.at[i, o - 1], ax2_rs.at[i, o - 1])
         if c == 0:
             weights[layer][2].wait()
-        hidden = hid[i].reshape(t, ff)
+        hidden = hid[i].reshape(t, -1)[:, :ff]
         for start, size in lane_tiles(d):
             branch = jnp.dot(hidden, wd[layer, :, start:start + size],
                              preferred_element_type=jnp.float32)
@@ -278,9 +329,11 @@
             final = strm[layer, c].astype(jnp.float32).reshape(t, d)
             out[c * t:(c + 1) * t, :] = final.astype(jnp.bfloat16)
 
-    steps = dict(u=u, x2=x2, h=h, g2=g2, wa=wa, wb=wb, sa=sa, sb=sb, sc=sc)
-    for name, layer, c in schedule(layers, chunks):
+    steps = dict(s=s, u=u, x2=x2, h=h, g2=g2, wa=wa, wb=wb, sa=sa, sb=sb, sc=sc)
+    for name, layer, c in schedule(layers, chunks, ny, nx, nz, t, ff, d):
         steps[name](layer, c)
+        if name == "wb" and c == chunks - 1 and layer + 1 < layers:
+            turn(layer + 1)
     for copy in pending:
         copy.wait_send()
 
@@ -293,7 +346,7 @@
     nx = nr // ny
     rows = tokens.shape[0]
     nz = nc // CORES
-    chunks = 2 if rows // 2 >= 16 * max(nr, nc) else 1
+    chunks = max(c for c in (1, 2, 4) if c == 1 or rows // c >= 8 * max(2 * nr, nc))
     t = rows // chunks
     n = layers * chunks
     cfg = (layers, chunks, ny, nx, nz, t, ff, d, d * nr)
@@ -301,6 +354,7 @@
     dma = pltpu.SemaphoreType.DMA
     vmem = pl.BlockSpec(memory_space=pltpu.VMEM)
     hbm = pl.BlockSpec(memory_space=pltpu.HBM)
+    wide = -(-ff // LANES) * LANES
     tz, tr = t // nc, t // nr
     px, py = max(nx - 1, 1), max(ny - 1, 1)
     return pl.pallas_call(
@@ -312,16 +366,17 @@
             pltpu.VMEM((layers, ff, d), bf16),
             pltpu.VMEM((layers, ff, d), bf16),
             pltpu.VMEM((layers, ff, d), bf16),
+            pltpu.VMEM((max(layers - 1, 1), 2, d, ff), bf16),
             pltpu.VMEM((layers, 2, 8 + t, ff), f32),
             pltpu.VMEM((n, 8, t), f32),
             pltpu.VMEM((n, nr - 1, 8, t), f32),
-            pltpu.VMEM((n, 2, ny, nx, tr, ff), bf16),
-            pltpu.VMEM((n, px, ny, tr, ff), bf16),
-            pltpu.VMEM((n, py, nx, tr, ff), bf16),
-            pltpu.VMEM((n, 2, max(px, py), tr, ff), bf16),
-            pltpu.VMEM((n, py, tr, ff), bf16),
-            pltpu.VMEM((n, px, tr, ff), bf16),
-            pltpu.VMEM((n, ny, nx, 2, tr // 2, ff), bf16),
+            pltpu.VMEM((n, 2, ny, nx, tr, wide), bf16),
+            pltpu.VMEM((n, px, ny, tr, wide), bf16),
+            pltpu.VMEM((n, py, nx, tr, wide), bf16),
+            pltpu.VMEM((n, 2, max(px, py), tr, wide), bf16),
+            pltpu.VMEM((n, py, tr, wide), bf16),
+            pltpu.VMEM((n, px, tr, wide), bf16),
+            pltpu.VMEM((n, ny, nx, 2, tr // 2, wide), bf16),
             pltpu.VMEM((chunks, CORES, t // CORES, d), f32),
             pltpu.VMEM((n, t // CORES, d), bf16),
             pltpu.VMEM((n, t // CORES, d), bf16),

time: 91.2 us -> 85.6 us (0.939)
  Pallas kernels: 89.2 us -> 83.4 us
    pallas_call x1, Pallas kernels: 89.2 us -> 83.4 us  [body(): pl.pallas_call(functools.partial(kernel, cfg), out_shape=jax.ShapeDtypeSt...]
where the time goes in v3:
time: 85.6 us; the launch traced here: 85.3 us
  Pallas kernels  83.4 us (97%)
  local copies, waits for them, and re-layouts  1.87 us (2%)
    pallas_call x1, Pallas kernels, body(): pl.pallas_call(functools.partial(kernel, cfg), out_shape=jax.ShapeDtypeSt...  83.4 us
    unnamed x1, local copies, waits for them, and re-layouts  1.87 us

profile of v3, /device:TPU:0, one launch (start us, length us, event | category | flops | bytes accessed | tf_op | source)
XLA Modules:
  0.0 85.3 jit_solution(4412734052533401056)
XLA Ops:
  0.0 83.4 %shard_map.73 = bf16[256,1024]{1,0:T(8,128)(2,1)} custom-call(bf16[256,1024]{1,0:T(8,128)(2,1)} %tokens.1, f32[2,1024]{1,0:T(2,128)} %gain.1, bf16[2,1376,1024]{2,1,0:T(8,128)(2,1)} %bitcast.4, bf16[2,1376,1024]{2,1,0:T(8,128)(2,1)} %bitcast.5, f32[3,2,1376]{2,1,0:T(2,128)} %bitcast.6, f32[3,2,1376]{2,1,0:T(2,128)} %bitcast.7, bf16[2,1376,1024]{2,1,0:T(8,128)(2,1)} %down_hbm.1), custom_call_target="tpu_custom_call" | custom-call | tf_op jit(solution)/shard_map/pallas_call | solution.py:360
  83.4 1.9 %copy.9 = bf16[256,1024]{1,0:T(8,128)(2,1)} copy(bf16[256,1024]{1,0:T(8,128)(2,1)} %shard_map.73) | data formatting | bytes 1048576
